TPU v7x, 32 devices: a whole 2x2x4 slice. The times are simulated.
32 devices in a mesh: ep: 8 (over z, core), tp: 4 (over y, x).
Axes of the slice: x: 2, y: 2, z: 4, core: 2. Of those that a mesh axis runs over, the one named last changes fastest.
Arguments:
- tokens: bfloat16 [256, 2560], P('ep'), may hold values from -6 to 6
- norm_gain: float32 [2560], replicated, may hold values from 0.1 to 1.9
- route: int32 [256, 4], P('ep'), may hold values from 0 to 7, all different within a row; in each aligned block of 32 rows (0 to 31, 32 to 63, ...) at most 24 rows name the same one
- route_weight: float32 [256, 4], P('ep'), may hold values from 0.1 to 1
- gate_weight: bfloat16 [8, 8960, 2560], P('ep', 'tp'), may hold values from -0.125 to 0.125
- up_weight: bfloat16 [8, 8960, 2560], P('ep', 'tp'), may hold values from -0.125 to 0.125
- down_weight: bfloat16 [8, 8960, 2560], P('ep', 'tp'), may hold values from -0.0625 to 0.0625
Outputs:
- mixed: bfloat16 [256, 2560], P('ep', 'tp')
Inputs may be any that keep to these rules, and one draw needn't show every extreme that they name: `route`: each row names 4 different experts. Among the rows of one index of ep no expert is named more than 24 times, a bound that some block reaches.
All inputs are finite; a program needn't handle non-finite values.
Results may differ from a plain program's by a relative error of at most 0.018.
Values may be sent and summed in bfloat16 or wider, within the bound.
A program may use at most 128 MiB of HBM per device.

v0:
```python
import jax
import jax.numpy as jnp
from jax import lax
from jax.sharding import PartitionSpec as P

epsilon = 1e-06


def on_device(tokens, norm_gain, route, route_weight, gate_weight, up_weight, down_weight):
    tok_rows, width = tokens.shape
    top_count = route.shape[1]
    local_experts = gate_weight.shape[0]
    ep_count = lax.axis_size("ep")
    tp_count = lax.axis_size("tp")
    experts = local_experts * ep_count
    capacity = min(tok_rows, max(2, (3 * tok_rows * top_count + 2 * experts - 1) // (2 * experts)))
    width_share = width // tp_count
    values = tokens.astype(jnp.float32)
    scaled = values * lax.rsqrt(jnp.mean(values * values, axis=-1, keepdims=True) + epsilon)
    normed = (scaled * norm_gain).astype(jnp.bfloat16)
    flat_route = route.reshape(tok_rows * top_count)
    onehot = (flat_route[:, None] == jnp.arange(experts, dtype=jnp.int32)[None, :]).astype(
        jnp.int32
    )
    slot_number = jnp.sum((jnp.cumsum(onehot, axis=0) - 1) * onehot, axis=-1)
    slot_index = flat_route * capacity + slot_number
    placing = (
        slot_index[None, :] == jnp.arange(experts * capacity, dtype=jnp.int32)[:, None]
    ).astype(jnp.bfloat16)
    repeated = jnp.repeat(normed, top_count, axis=0)
    columns = lax.dynamic_slice_in_dim(repeated, lax.axis_index("tp") * width_share, width_share, 1)
    send = jnp.dot(placing, columns, preferred_element_type=jnp.float32).astype(jnp.bfloat16)
    send = send.reshape(ep_count, local_experts, capacity, width_share)
    arrived = lax.all_to_all(send, "ep", split_axis=0, concat_axis=0, tiled=True)
    piece = lax.all_gather(arrived, "tp", axis=3, tiled=True)
    gate = jnp.einsum("sjcd,jfd->sjcf", piece, gate_weight, preferred_element_type=jnp.float32)
    upward = jnp.einsum("sjcd,jfd->sjcf", piece, up_weight, preferred_element_type=jnp.float32)
    hidden = (jax.nn.silu(gate) * upward).astype(jnp.bfloat16)
    partial_value = jnp.einsum(
        "sjcf,jfd->sjcd", hidden, down_weight, preferred_element_type=jnp.float32
    )
    shares = lax.psum_scatter(
        partial_value.astype(jnp.bfloat16), "tp", scatter_dimension=3, tiled=True
    )
    returned = lax.all_to_all(shares, "ep", split_axis=0, concat_axis=0, tiled=True)
    results = returned.reshape(experts * capacity, width_share)
    picked = results[slot_index].reshape(tok_rows, top_count, width_share).astype(jnp.float32)
    mixed = jnp.sum(route_weight[:, :, None] * picked, axis=1)
    return mixed.astype(jnp.bfloat16)


def solution(mesh):
    placed = (
        P("ep", None),
        P(),
        P("ep", None),
        P("ep", None),
        P("ep", "tp", None),
        P("ep", "tp", None),
        P("ep", "tp", None),
    )
    return jax.shard_map(
        on_device, mesh=mesh, in_specs=placed, out_specs=P("ep", "tp"), check_vma=False
    )
```

profile of v0, /device:TPU:0, one launch (start us, length us, event | category | flops | bytes accessed | tf_op | source)
XLA Modules:
  0.0 130.7 jit_solution(8233798995752015378)
XLA Ops:
  6.5 0.8 copy.15
  7.3 0.1 reshape.82
  7.4 0.1 fusion.37
  7.5 0.2 reduce_window_sum.11
  7.7 0.2 select_reduce_fusion
  7.9 1.1 fusion.33
  8.9 1.0 fusion.35
  10.0 0.2 broadcast_in_dim.2
  10.1 0.1 reshape.83
  10.3 0.2 convolution_convert_fusion
  10.5 15.5 %all_to_all.10 = bf16[8,1,24,640]{3,2,1,0:T(8,128)(2,1)S(1)} all-to-all(bf16[8,1,24,640]{3,2,1,0:T(8,128)(2,1)S(1)} %bitcast.85), channel_id=1, replica_groups=mesh['ep'=8,'tp'=4] {'ep'}, dimensions={0} | all-to-all | bytes 491520 | tf_op jit(solution)/shard_map/all_to_all | solution.py:34
  26.0 13.9 %all_gather.3 = bf16[8,1,24,2560]{3,2,0,1:T(8,128)(2,1)S(1)} all-gather(bf16[8,1,24,640]{3,2,0,1:T(8,128)(2,1)S(1)} %bitcast.84), channel_id=1, replica_groups=mesh['ep'=8,'tp'=4] {'tp'}, dimensions={3}, use_global_device_ids=true | all-gather | bytes 1228800 | tf_op jit(solution)/shard_map/all_gather | solution.py:35
  39.9 9.2 %fusion.6 = f32[8,1,24,2240]{3,2,0,1:T(8,128)} fusion(bf16[1,2240,2560]{2,1,0:T(8,128)(2,1)} %param.11, bf16[8,1,24,2560]{3,2,0,1:T(8,128)(2,1)S(1)} %all_gather.3), kind=kOutput, calls=%fused_computation.7 | convolution fusion | flops 2202009600 | bytes 14172160 | tf_op jit(solution)/shard_map/sjcd,jfd->sjcf/dot_general | solution.py:36
  49.1 14.7 %fusion.24 = bf16[8,1,24,2560]{3,2,0,1:T(8,128)(2,1)S(1)} fusion(bf16[1,2240,2560]{2,1,0:T(8,128)(2,1)} %param.13, bf16[1,2240,2560]{2,1,0:T(8,128)(2,1)} %param.12, f32[8,1,24,2240]{3,2,0,1:T(8,128)} %fusion.6, bf16[8,1,24,2560]{3,2,0,1:T(8,128)(2,1)S(1)} %all_gather.3), kind=kOutput, calls=%fused_computation.13 | convolution fusion | flops 4407091200 | bytes 26624000 | tf_op jit(solution)/shard_map/sjcf,jfd->sjcd/dot_general | solution.py:39
  63.8 4.6 %copy.20 = bf16[8,1,24,2560]{2,0,1,3:T(8,128)(2,1)} copy(bf16[8,1,24,2560]{3,2,0,1:T(8,128)(2,1)S(1)} %fusion.24) | data formatting | bytes 1966080
  68.4 7.3 %reshape.103 = bf16[2560,192]{1,0:T(8,128)(2,1)} reshape(bf16[2560,1,8,24]{3,2,1,0:T(8,128)(2,1)} %bitcast.81) | data formatting | bytes 1966080
  75.7 28.7 %reduce-scatter.4.cloned.1.call-done = bf16[640,192]{1,0:T(8,128)(2,1)} async-done(((bf16[2560,192]{1,0:T(8,128)(2,1)}), bf16[640,192]{1,0:T(8,128)(2,1)}) %reduce-scatter.4.cloned.1.call-update) | async-done | bytes 245776
  104.5 2.0 %reshape.104 = bf16[640,1,8,24]{3,2,1,0:T(8,128)(2,1)S(1)} reshape(bf16[640,192]{1,0:T(8,128)(2,1)} %reduce-scatter.4.cloned.1.call-done) | data formatting | bytes 491520
  106.5 1.5 %copy.21 = bf16[8,1,24,640]{3,2,0,1:T(8,128)(2,1)} copy(bf16[8,1,24,640]{2,0,1,3:T(8,128)(2,1)S(1)} %bitcast.83) | data formatting | bytes 491520
  108.0 4.6 %all-to-all-start.1 = ((bf16[8,1,24,640]{3,2,1,0:T(8,128)(2,1)}), bf16[8,1,24,640]{3,2,1,0:T(8,128)(2,1)S(1)}, u32[]{:S(2)}, u32[]{:S(2)}) async-start(bf16[8,1,24,640]{3,2,1,0:T(8,128)(2,1)} %bitcast.22), calls=%async_computation.1 | async-start | bytes 491520 | tf_op jit(solution)/shard_map/all_to_all | solution.py:45
  112.7 0.1 mul.78
  112.9 9.0 %all-to-all-done.1 = bf16[8,1,24,640]{3,2,1,0:T(8,128)(2,1)S(1)} async-done(((bf16[8,1,24,640]{3,2,1,0:T(8,128)(2,1)}), bf16[8,1,24,640]{3,2,1,0:T(8,128)(2,1)S(1)}, u32[]{:S(2)}, u32[]{:S(2)}) %all-to-all-start.1) | async-done | bytes 245792 | tf_op jit(solution)/shard_map/all_to_all | solution.py:45
  121.9 0.9 gather_fusion
  122.9 0.9 multiply_reduce_fusion
  (14 shorter events, 0.3 us)
Async XLA Ops:
  6.5 97.9 %reduce-scatter.4.cloned.1.call-start = ((), (), s32[]{:S(2)}) async-start(), calls=%async_computation.3 | async-start | bytes 1638400
  75.7 36.9 %copy-start = (s32[32,4]{0,1:T(4,128)S(1)}, s32[32,4]{0,1:T(4,128)}, u32[]{:S(2)}) copy-start(s32[32,4]{0,1:T(4,128)} %param.9) | copy-start | bytes 1540
  75.7 37.1 %copy-start.1 = (f32[32,4]{0,1:T(4,128)S(1)}, f32[32,4]{0,1:T(4,128)}, u32[]{:S(2)}) copy-start(f32[32,4]{0,1:T(4,128)} %param.10) | copy-start | bytes 1540
  108.0 14.0 %all-to-all-start.1 = ((bf16[8,1,24,640]{3,2,1,0:T(8,128)(2,1)}), bf16[8,1,24,640]{3,2,1,0:T(8,128)(2,1)S(1)}, u32[]{:S(2)}, u32[]{:S(2)}) async-start(bf16[8,1,24,640]{3,2,1,0:T(8,128)(2,1)} %bitcast.22), calls=%async_computation.1 | async-start | bytes 491520 | tf_op jit(solution)/shard_map/all_to_all | solution.py:45
Sparse Core Ops, SparseCore 0:
  75.8 28.5 reduce-scatter.3
where the time goes:
time: 131 us
  waiting for transfers between devices  37.8 us (29%)
  blocking collectives  29.4 us (22%)
  matrix products  24.1 us (18%)
  local copies, waits for them, and re-layouts  17.8 us (14%)
  between operations  13.5 us (10%)
  starting transfers between devices  4.61 us (4%)
  other arithmetic  3.44 us (3%)
    unnamed x2, waiting for transfers between devices  28.8 us
    unnamed x10, local copies, waits for them, and re-layouts  16.2 us
    all_to_all x1, blocking collectives, on_device(): lax.all_to_all(send, 'ep', split_axis=0, concat_axis=0, tiled=True)  15.5 us
    dot_general x1, matrix products, on_device(): jnp.einsum('sjcf,jfd->sjcd', hidden, down_weight, preferred_element_type=...  14.7 us
    all_gather x1, blocking collectives, on_device(): piece = lax.all_gather(arrived, 'tp', axis=3, tiled=True)  13.9 us
    dot_general x1, matrix products, on_device(): jnp.einsum('sjcd,jfd->sjcf', piece, gate_weight, preferred_element_type=j...  9.21 us
    all_to_all x1, waiting for transfers between devices, on_device(): lax.all_to_all(shares, 'ep', split_axis=0, concat_axis=0, tiled=True)  9.04 us
    all_to_all x1, starting transfers between devices, on_device(): lax.all_to_all(shares, 'ep', split_axis=0, concat_axis=0, tiled=True)  4.6 us
  transfers between devices with their start and end apart: 2, of which 2 were waited for; matrix products, arithmetic and copies ran while one was open for 0% of the time, Pallas kernels for 0%

commit v1 on v0

--- a/solution.py
+++ b/solution.py
@@ -4,6 +4,20 @@
 from jax.sharding import PartitionSpec as P
 
 epsilon = 1e-06
+
+
+def raise_the_runs(m, dim_k, mine_x):
+    then, before = (m.shape[:dim_k], m.shape[dim_k + 1 :])
+    state_now = m.reshape(*then, mine_x, -1, *before)
+    left_arr = jnp.moveaxis(state_now, dim_k, 0)
+    return left_arr
+
+
+def bind_tails_for(mat, dim_no):
+    mat = jnp.moveaxis(mat, 0, dim_no)
+    a_now = mat.shape
+    answer = mat.reshape(*a_now[:dim_no], a_now[dim_no] * a_now[dim_no + 1], *a_now[dim_no + 2 :])
+    return answer
 
 
 def on_device(tokens, norm_gain, route, route_weight, gate_weight, up_weight, down_weight):
@@ -31,7 +45,18 @@
     columns = lax.dynamic_slice_in_dim(repeated, lax.axis_index("tp") * width_share, width_share, 1)
     send = jnp.dot(placing, columns, preferred_element_type=jnp.float32).astype(jnp.bfloat16)
     send = send.reshape(ep_count, local_experts, capacity, width_share)
-    arrived = lax.all_to_all(send, "ep", split_axis=0, concat_axis=0, tiled=True)
+    v_next = lax.axis_size("ep")
+    outer = lax.axis_index("ep")
+    formed, x_now = (v_next, outer)
+    x_next = raise_the_runs(send, 0, formed)
+    kept_rows = [x_next[x_now]]
+    for num in range(1, formed):
+        val2 = x_next[x_now ^ num]
+        reply = lax.ppermute(val2, "ep", [(it, it ^ num) for it in range(formed)])
+        kept_rows.append(reply)
+    upper = jnp.stack(kept_rows, 0)
+    x_next = upper[x_now ^ jnp.arange(formed)]
+    arrived = bind_tails_for(x_next, 0)
     piece = lax.all_gather(arrived, "tp", axis=3, tiled=True)
     gate = jnp.einsum("sjcd,jfd->sjcf", piece, gate_weight, preferred_element_type=jnp.float32)
     upward = jnp.einsum("sjcd,jfd->sjcf", piece, up_weight, preferred_element_type=jnp.float32)

time: 131 us -> 131 us (level)
  blocking collectives: 29.4 us -> 15.2 us
  starting transfers between devices: 4.61 us -> 14.4 us
  waiting for transfers between devices: 37.8 us -> 41 us
    all_to_all x1 -> x0, blocking collectives: 15.5 us -> none  [on_device(): lax.all_to_all(send, 'ep', split_axis=0, concat_axis=0, tiled=True)]
    ppermute x0 -> x7, starting transfers between devices: none -> 9.8 us  [on_device(): reply = lax.ppermute(val2, 'ep', [(it, it ^ num) for it in range(formed)])]
    ppermute x0 -> x7, waiting for transfers between devices: none -> 4.99 us  [on_device(): reply = lax.ppermute(val2, 'ep', [(it, it ^ num) for it in range(formed)])]
    unnamed x2, waiting for transfers between devices: 28.8 us -> 27 us
    all_gather x1, blocking collectives: 13.9 us -> 15.2 us  [on_device(): piece = lax.all_gather(arrived, 'tp', axis=3, tiled=True)]
    unnamed x10 -> x16, local copies, waits for them, and re-layouts: 16.2 us -> 16.3 us
  transfers between devices with their start and end apart: 2 -> 9, of which waited for: 2 -> 5; matrix products, arithmetic and copies ran while one was open for 0% -> 0% of each run, Pallas kernels for 0% -> 0%
where the time goes in v1:
time: 131 us; the launch traced here: 130 us
  waiting for transfers between devices  41 us (31%)
  matrix products  24.1 us (18%)
  local copies, waits for them, and re-layouts  18.5 us (14%)
  blocking collectives  15.2 us (12%)
  starting transfers between devices  14.4 us (11%)
  between operations  13.6 us (10%)
  other arithmetic  3.45 us (3%)
    unnamed x2, waiting for transfers between devices  27 us
    unnamed x16, local copies, waits for them, and re-layouts  16.3 us
    all_gather x1, blocking collectives, on_device(): piece = lax.all_gather(arrived, 'tp', axis=3, tiled=True)  15.2 us
    dot_general x1, matrix products, on_device(): jnp.einsum('sjcf,jfd->sjcd', hidden, down_weight, preferred_element_type=...  14.7 us
    ppermute x7, starting transfers between devices, on_device(): reply = lax.ppermute(val2, 'ep', [(it, it ^ num) for it in range(formed)])  9.8 us
    dot_general x1, matrix products, on_device(): jnp.einsum('sjcd,jfd->sjcf', piece, gate_weight, preferred_element_type=j...  9.22 us
    all_to_all x1, waiting for transfers between devices, on_device(): lax.all_to_all(shares, 'ep', split_axis=0, concat_axis=0, tiled=True)  9.04 us
    ppermute x7, waiting for transfers between devices, on_device(): reply = lax.ppermute(val2, 'ep', [(it, it ^ num) for it in range(formed)])  4.99 us
  transfers between devices with their start and end apart: 9, of which 5 were waited for; matrix products, arithmetic and copies ran while one was open for 0% of the time, Pallas kernels for 0%

profile of v1, /device:TPU:0, one launch (start us, length us, event | category | flops | bytes accessed | tf_op | source)
XLA Modules:
  0.0 130.4 jit_solution(8765678444650808613)
XLA Ops:
  6.5 0.8 copy.15
  7.9 1.1 fusion.30
  8.9 1.0 fusion.32
  10.3 0.2 convolution_convert_fusion
  10.6 0.6 collective-permute-start
  11.2 2.6 %collective-permute-start.1 = (bf16[1,1,24,640]{3,2,1,0:T(8,128)(2,1)S(1)}, bf16[1,1,24,640]{3,2,1,0:T(8,128)(2,1)S(1)}, u32[]{:S(2)}, u32[]{:S(2)}) collective-permute-start(bf16[1,1,24,640]{3,2,1,0:T(8,128)(2,1)S(1)} %get-tuple-element.10), channel_id=1, source_target_pairs={{0,8},{4,12},{8,0},{12,4},{16,24},{20,28},{24,16},{28,20},{1,9},{5... | collective-permute-start | bytes 92168 | tf_op jit(solution)/shard_map/ppermute | solution.py:55
  13.8 2.8 %collective-permute-start.3 = (bf16[1,1,24,640]{3,2,1,0:T(8,128)(2,1)S(1)}, bf16[1,1,24,640]{3,2,1,0:T(8,128)(2,1)S(1)}, u32[]{:S(2)}, u32[]{:S(2)}) collective-permute-start(bf16[1,1,24,640]{3,2,1,0:T(8,128)(2,1)S(1)} %get-tuple-element.8), channel_id=1, source_target_pairs={{0,16},{4,20},{8,24},{12,28},{16,0},{20,4},{24,8},{28,12},{1,17},{... | collective-permute-start | bytes 92168 | tf_op jit(solution)/shard_map/ppermute | solution.py:55
  16.6 3.7 %collective-permute-start.5 = (bf16[1,1,24,640]{3,2,1,0:T(8,128)(2,1)S(1)}, bf16[1,1,24,640]{3,2,1,0:T(8,128)(2,1)S(1)}, u32[]{:S(2)}, u32[]{:S(2)}) collective-permute-start(bf16[1,1,24,640]{3,2,1,0:T(8,128)(2,1)S(1)} %get-tuple-element.6), channel_id=1, source_target_pairs={{0,24},{4,28},{8,16},{12,20},{16,8},{20,12},{24,0},{28,4},{1,25},{... | collective-permute-start | bytes 92168 | tf_op jit(solution)/shard_map/ppermute | solution.py:55
  20.5 0.4 collective-permute-done.4
  20.9 2.0 %collective-permute-done.5 = bf16[1,1,24,640]{3,2,1,0:T(8,128)(2,1)S(1)} collective-permute-done((bf16[1,1,24,640]{3,2,1,0:T(8,128)(2,1)S(1)}, bf16[1,1,24,640]{3,2,1,0:T(8,128)(2,1)S(1)}, u32[]{:S(2)}, u32[]{:S(2)}) %collective-permute-start.5) | collective-permute-done | bytes 30752 | tf_op jit(solution)/shard_map/ppermute | solution.py:55
  22.9 2.6 %collective-permute-done.6 = bf16[1,1,24,640]{3,2,1,0:T(8,128)(2,1)S(1)} collective-permute-done((bf16[1,1,24,640]{3,2,1,0:T(8,128)(2,1)S(1)}, bf16[1,1,24,640]{3,2,1,0:T(8,128)(2,1)S(1)}, u32[]{:S(2)}, u32[]{:S(2)}) %collective-permute-start.6) | collective-permute-done | bytes 30752 | tf_op jit(solution)/shard_map/ppermute | solution.py:55
  25.5 0.6 gather_fusion
  26.1 15.2 %all-gather = bf16[8,24,2560]{2,1,0:T(8,128)(2,1)S(1)} all-gather(bf16[8,24,640]{2,1,0:T(8,128)(2,1)S(1)} %gather_fusion), channel_id=2, replica_groups=mesh['ep'=8,'tp'=4] {'tp'}, dimensions={2}, use_global_device_ids=true | all-gather | bytes 1228800 | tf_op jit(solution)/shard_map/all_gather | solution.py:60
  41.3 9.2 %fusion.6 = f32[8,1,24,2240]{3,2,0,1:T(8,128)} fusion(bf16[8,24,2560]{2,1,0:T(8,128)(2,1)S(1)} %all-gather, bf16[1,2240,2560]{2,1,0:T(8,128)(2,1)} %param.11), kind=kOutput, calls=%fused_computation.8 | convolution fusion | flops 2202009600 | bytes 14172160 | tf_op jit(solution)/shard_map/sjcd,jfd->sjcf/dot_general | solution.py:61
  50.5 14.7 %fusion.24 = bf16[8,1,24,2560]{3,2,0,1:T(8,128)(2,1)S(1)} fusion(bf16[1,2240,2560]{2,1,0:T(8,128)(2,1)} %param.13, bf16[8,24,2560]{2,1,0:T(8,128)(2,1)S(1)} %all-gather, bf16[1,2240,2560]{2,1,0:T(8,128)(2,1)} %param.12, f32[8,1,24,2240]{3,2,0,1:T(8,128)} %fusion.6), kind=kOutput, calls=%fused_computation.14 | convolution fusion | flops 4407091200 | bytes 26624000 | tf_op jit(solution)/shard_map/sjcf,jfd->sjcd/dot_general | solution.py:64
  65.3 4.6 %copy.18 = bf16[8,1,24,2560]{2,0,1,3:T(8,128)(2,1)} copy(bf16[8,1,24,2560]{3,2,0,1:T(8,128)(2,1)S(1)} %fusion.24) | data formatting | bytes 1966080
  69.8 7.3 %reshape.134 = bf16[2560,192]{1,0:T(8,128)(2,1)} reshape(bf16[2560,1,8,24]{3,2,1,0:T(8,128)(2,1)} %bitcast.105) | data formatting | bytes 1966080
  77.2 27.0 %reduce-scatter.4.cloned.1.call-done = bf16[640,192]{1,0:T(8,128)(2,1)} async-done(((bf16[2560,192]{1,0:T(8,128)(2,1)}), bf16[640,192]{1,0:T(8,128)(2,1)}) %reduce-scatter.4.cloned.1.call-update) | async-done | bytes 245776
  104.2 2.0 %reshape.135 = bf16[640,1,8,24]{3,2,1,0:T(8,128)(2,1)S(1)} reshape(bf16[640,192]{1,0:T(8,128)(2,1)} %reduce-scatter.4.cloned.1.call-done) | data formatting | bytes 491520
  106.2 1.5 %copy.19 = bf16[8,1,24,640]{3,2,0,1:T(8,128)(2,1)} copy(bf16[8,1,24,640]{2,0,1,3:T(8,128)(2,1)S(1)} %bitcast.107) | data formatting | bytes 491520
  107.7 4.6 %all-to-all-start = ((bf16[8,1,24,640]{3,2,1,0:T(8,128)(2,1)}), bf16[8,1,24,640]{3,2,1,0:T(8,128)(2,1)S(1)}, u32[]{:S(2)}, u32[]{:S(2)}) async-start(bf16[8,1,24,640]{3,2,1,0:T(8,128)(2,1)} %bitcast.35), calls=%async_computation | async-start | bytes 491520 | tf_op jit(solution)/shard_map/all_to_all | solution.py:70
  112.6 9.0 %all-to-all-done = bf16[8,1,24,640]{3,2,1,0:T(8,128)(2,1)S(1)} async-done(((bf16[8,1,24,640]{3,2,1,0:T(8,128)(2,1)}), bf16[8,1,24,640]{3,2,1,0:T(8,128)(2,1)S(1)}, u32[]{:S(2)}, u32[]{:S(2)}) %all-to-all-start) | async-done | bytes 245792 | tf_op jit(solution)/shard_map/all_to_all | solution.py:70
  121.7 0.9 gather_fusion.1
  122.6 0.9 multiply_reduce_fusion
  (38 shorter events, 1.6 us)
Async XLA Ops:
  6.5 97.6 %reduce-scatter.4.cloned.1.call-start = ((), (), s32[]{:S(2)}) async-start(), calls=%async_computation.2 | async-start | bytes 1638400
  10.6 6.0 %collective-permute-start = (bf16[1,1,24,640]{3,2,1,0:T(8,128)(2,1)S(1)}, bf16[1,1,24,640]{3,2,1,0:T(8,128)(2,1)S(1)}, u32[]{:S(2)}, u32[]{:S(2)}) collective-permute-start(bf16[1,1,24,640]{3,2,1,0:T(8,128)(2,1)S(1)} %get-tuple-element.11), channel_id=1, source_target_pairs={{0,4},{4,0},{8,12},{12,8},{16,20},{20,16},{24,28},{28,24},{1,5},{5... | collective-permute-start | bytes 92168 | tf_op jit(solution)/shard_map/ppermute | solution.py:55
  11.2 9.2 %collective-permute-start.1 = (bf16[1,1,24,640]{3,2,1,0:T(8,128)(2,1)S(1)}, bf16[1,1,24,640]{3,2,1,0:T(8,128)(2,1)S(1)}, u32[]{:S(2)}, u32[]{:S(2)}) collective-permute-start(bf16[1,1,24,640]{3,2,1,0:T(8,128)(2,1)S(1)} %get-tuple-element.10), channel_id=1, source_target_pairs={{0,8},{4,12},{8,0},{12,4},{16,24},{20,28},{24,16},{28,20},{1,9},{5... | collective-permute-start | bytes 92168 | tf_op jit(solution)/shard_map/ppermute | solution.py:55
  13.8 6.7 %collective-permute-start.2 = (bf16[1,1,24,640]{3,2,1,0:T(8,128)(2,1)S(1)}, bf16[1,1,24,640]{3,2,1,0:T(8,128)(2,1)S(1)}, u32[]{:S(2)}, u32[]{:S(2)}) collective-permute-start(bf16[1,1,24,640]{3,2,1,0:T(8,128)(2,1)S(1)} %get-tuple-element.9), channel_id=1, source_target_pairs={{0,12},{4,8},{8,4},{12,0},{16,28},{20,24},{24,20},{28,16},{1,13},{... | collective-permute-start | bytes 92168 | tf_op jit(solution)/shard_map/ppermute | solution.py:55
  13.8 6.6 %collective-permute-start.3 = (bf16[1,1,24,640]{3,2,1,0:T(8,128)(2,1)S(1)}, bf16[1,1,24,640]{3,2,1,0:T(8,128)(2,1)S(1)}, u32[]{:S(2)}, u32[]{:S(2)}) collective-permute-start(bf16[1,1,24,640]{3,2,1,0:T(8,128)(2,1)S(1)} %get-tuple-element.8), channel_id=1, source_target_pairs={{0,16},{4,20},{8,24},{12,28},{16,0},{20,4},{24,8},{28,12},{1,17},{... | collective-permute-start | bytes 92168 | tf_op jit(solution)/shard_map/ppermute | solution.py:55
  16.6 4.3 %collective-permute-start.4 = (bf16[1,1,24,640]{3,2,1,0:T(8,128)(2,1)S(1)}, bf16[1,1,24,640]{3,2,1,0:T(8,128)(2,1)S(1)}, u32[]{:S(2)}, u32[]{:S(2)}) collective-permute-start(bf16[1,1,24,640]{3,2,1,0:T(8,128)(2,1)S(1)} %get-tuple-element.7), channel_id=1, source_target_pairs={{0,20},{4,16},{8,28},{12,24},{16,4},{20,0},{24,12},{28,8},{1,21},{... | collective-permute-start | bytes 92168 | tf_op jit(solution)/shard_map/ppermute | solution.py:55
  16.6 6.3 %collective-permute-start.5 = (bf16[1,1,24,640]{3,2,1,0:T(8,128)(2,1)S(1)}, bf16[1,1,24,640]{3,2,1,0:T(8,128)(2,1)S(1)}, u32[]{:S(2)}, u32[]{:S(2)}) collective-permute-start(bf16[1,1,24,640]{3,2,1,0:T(8,128)(2,1)S(1)} %get-tuple-element.6), channel_id=1, source_target_pairs={{0,24},{4,28},{8,16},{12,20},{16,8},{20,12},{24,0},{28,4},{1,25},{... | collective-permute-start | bytes 92168 | tf_op jit(solution)/shard_map/ppermute | solution.py:55
  20.3 5.2 %collective-permute-start.6 = (bf16[1,1,24,640]{3,2,1,0:T(8,128)(2,1)S(1)}, bf16[1,1,24,640]{3,2,1,0:T(8,128)(2,1)S(1)}, u32[]{:S(2)}, u32[]{:S(2)}) collective-permute-start(bf16[1,1,24,640]{3,2,1,0:T(8,128)(2,1)S(1)} %get-tuple-element.5), channel_id=1, source_target_pairs={{0,28},{4,24},{8,20},{12,16},{16,12},{20,8},{24,4},{28,0},{1,29},{... | collective-permute-start | bytes 92168 | tf_op jit(solution)/shard_map/ppermute | solution.py:55
  77.2 35.2 %copy-start = (s32[32,4]{0,1:T(4,128)S(1)}, s32[32,4]{0,1:T(4,128)}, u32[]{:S(2)}) copy-start(s32[32,4]{0,1:T(4,128)} %param.9) | copy-start | bytes 1540
  77.2 35.4 %copy-start.1 = (f32[32,4]{0,1:T(4,128)S(1)}, f32[32,4]{0,1:T(4,128)}, u32[]{:S(2)}) copy-start(f32[32,4]{0,1:T(4,128)} %param.10) | copy-start | bytes 1540
  107.7 14.0 %all-to-all-start = ((bf16[8,1,24,640]{3,2,1,0:T(8,128)(2,1)}), bf16[8,1,24,640]{3,2,1,0:T(8,128)(2,1)S(1)}, u32[]{:S(2)}, u32[]{:S(2)}) async-start(bf16[8,1,24,640]{3,2,1,0:T(8,128)(2,1)} %bitcast.35), calls=%async_computation | async-start | bytes 491520 | tf_op jit(solution)/shard_map/all_to_all | solution.py:70
Sparse Core Ops, SparseCore 0:
  77.3 26.8 reduce-scatter.3
